TPU v7x, 32 devices: a whole 2x2x4 slice. The times are simulated.
32 devices in a mesh: dp: 4 (over y, x), kv: 4 (over z), tp: 2 (over core).
Axes of the slice: x: 2, y: 2, z: 4, core: 2. Of those that a mesh axis runs over, the one named last changes fastest.
Arguments:
- tokens: bfloat16 [128, 2048], P('dp', ('kv', 'tp')), may hold values from -60 to 60
- first_norm_gain: float32 [2048], replicated, may hold values from 0.1 to 1.9
- first_gate_weight: bfloat16 [2048, 5632], P(None, ('kv', 'tp')), may hold values from -0.125 to 0.125
- first_up_weight: bfloat16 [2048, 5632], P(None, ('kv', 'tp')), may hold values from -0.125 to 0.125
- first_down_weight: bfloat16 [5632, 2048], P(('kv', 'tp')), may hold values from -0.109375 to 0.109375
- mixer_norm_gain: float32 [2048], replicated, may hold values from 0.1 to 1.9
- query_weight: bfloat16 [2048, 1024], P('kv', 'tp'), may hold values from -0.125 to 0.125
- key_weight: bfloat16 [2048, 1024], P('kv', 'tp'), may hold values from -0.125 to 0.125
- value_weight: bfloat16 [2048, 1024], P('kv', 'tp'), may hold values from -0.125 to 0.125
- output_gate_weight: bfloat16 [2048, 1024], P('kv', 'tp'), may hold values from -0.125 to 0.125
- strength_weight: bfloat16 [2048, 8], replicated, may hold values from -0.125 to 0.125
- decay_weight: bfloat16 [2048, 8], replicated, may hold values from -0.125 to 0.125
- head_decay_log: float32 [8], replicated, may hold values from 0 to 2.77
- decay_input_bias: float32 [8], replicated, may hold values from -4 to 0
- decay_extra_log: float32 [128, 8], P(('dp', 'kv'), 'tp'), may hold values from -0.7 to 0
- head_norm_gain: float32 [128], replicated, may hold values from 0.1 to 1.9
- state: float32 [128, 8, 128, 128], P(('dp', 'kv'), 'tp'), may hold values from -0.6 to 0.6
- mixer_output_weight: bfloat16 [1024, 2048], P('tp', 'kv'), may hold values from -0.1875 to 0.1875
- second_norm_gain: float32 [2048], replicated, may hold values from 0.1 to 1.9
- second_gate_weight: bfloat16 [2048, 5632], P(None, ('kv', 'tp')), may hold values from -0.125 to 0.125
- second_up_weight: bfloat16 [2048, 5632], P(None, ('kv', 'tp')), may hold values from -0.125 to 0.125
- second_down_weight: bfloat16 [5632, 2048], P(('kv', 'tp')), may hold values from -0.109375 to 0.109375
Outputs:
- layer_out: bfloat16 [128, 2048], P('dp', ('kv', 'tp'))
- new_state: float32 [128, 8, 128, 128], P(('dp', 'kv'), 'tp')
All inputs are finite; a program needn't handle non-finite values.
Results may differ from a plain program's by a relative error of at most 0.014.
Values may be sent and summed in bfloat16 or wider, within the bound.
A program may use at most 64 MiB of HBM per device.

v0:
```python
import jax
import jax.numpy as jnp
from jax import lax
from jax.sharding import PartitionSpec as P

EPS = 1e-06


def row_scale(values):
    return lax.rsqrt(jnp.mean(values * values, axis=-1, keepdims=True) + EPS)


def unit_rows(values):
    return values * lax.rsqrt(jnp.sum(values * values, axis=-1, keepdims=True) + EPS)


def block_terms(row_data, gain_vec, w_gate, w_up, w_down):
    rows32 = row_data.astype(jnp.float32)
    normed = (rows32 * row_scale(rows32) * gain_vec).astype(jnp.bfloat16)
    gate_pre = jnp.dot(normed, w_gate, preferred_element_type=jnp.float32)
    upward = jnp.dot(normed, w_up, preferred_element_type=jnp.float32)
    hidden = (jax.nn.silu(gate_pre) * upward).astype(jnp.bfloat16)
    return jnp.dot(hidden, w_down, preferred_element_type=jnp.float32)


def delta_step(
    query_vec, key_vec, value_vec, gate_vals, beta_gate, head_decay_rate, state, head_norm_gain
):
    recalled = jnp.einsum("shd,shde->she", key_vec, state, precision=lax.Precision.HIGHEST)
    correction = beta_gate[..., None] * (value_vec - head_decay_rate[..., None] * recalled)
    new_state = (
        head_decay_rate[..., None, None] * state + key_vec[..., :, None] * correction[..., None, :]
    )
    read_out = jnp.einsum("shd,shde->she", query_vec, new_state, precision=lax.Precision.HIGHEST)
    normed = read_out * row_scale(read_out) * head_norm_gain
    return (normed * jax.nn.silu(gate_vals), new_state)


def shards(
    tokens,
    first_norm_gain,
    first_gate_weight,
    first_up_weight,
    first_down_weight,
    mixer_norm_gain,
    query_weight,
    key_weight,
    value_weight,
    output_gate_weight,
    strength_weight,
    decay_weight,
    head_decay_log,
    decay_input_bias,
    decay_extra_log,
    head_norm_gain,
    state,
    mixer_output_weight,
    second_norm_gain,
    second_gate_weight,
    second_up_weight,
    second_down_weight,
):
    batch_rows, columns = tokens.shape
    kv_index = lax.axis_index("kv")
    tp_index = lax.axis_index("tp")
    own_block = kv_index * lax.axis_size("tp") + tp_index
    seq_dev, heads_dev, head_size = (state.shape[0], state.shape[1], state.shape[2])
    kv_width = query_weight.shape[0]
    head_cols = heads_dev * head_size
    model_width = mixer_norm_gain.shape[0]
    rows_all = lax.all_gather(tokens, ("kv", "tp"), axis=1, tiled=True)
    ffn_terms = block_terms(
        rows_all, first_norm_gain, first_gate_weight, first_up_weight, first_down_weight
    )
    share_sum = lax.psum_scatter(
        ffn_terms.astype(jnp.bfloat16), ("kv", "tp"), scatter_dimension=1, tiled=True
    ).astype(jnp.float32)
    first_rows = (tokens.astype(jnp.float32) + 0.5 * share_sum).astype(jnp.bfloat16)
    first32 = first_rows.astype(jnp.float32)
    kv_block = lax.all_gather(first_rows, "tp", axis=1, tiled=True)
    own_gain = lax.dynamic_slice_in_dim(mixer_norm_gain, own_block * columns, columns)
    own_scaled = (first32 * own_gain).astype(jnp.bfloat16)
    beta_rows = lax.dynamic_slice_in_dim(strength_weight, own_block * columns, columns, 0)
    decay_rows = lax.dynamic_slice_in_dim(decay_weight, own_block * columns, columns, 0)
    squares, beta_pre, decay_logits = lax.psum(
        (
            jnp.sum(first32 * first32, axis=1),
            jnp.dot(own_scaled, beta_rows, preferred_element_type=jnp.float32),
            jnp.dot(own_scaled, decay_rows, preferred_element_type=jnp.float32),
        ),
        ("kv", "tp"),
    )
    row_factor = lax.rsqrt(squares / model_width + EPS)
    block_gain = lax.dynamic_slice_in_dim(mixer_norm_gain, kv_index * kv_width, kv_width)
    block_scaled = (kv_block.astype(jnp.float32) * block_gain).astype(jnp.bfloat16)
    projected = lax.psum_scatter(
        jnp.concatenate(
            [
                jnp.dot(block_scaled, weight, preferred_element_type=jnp.float32)
                for weight in (query_weight, key_weight, value_weight, output_gate_weight)
            ],
            axis=1,
        ).astype(jnp.bfloat16),
        "kv",
        scatter_dimension=0,
        tiled=True,
    ).astype(jnp.float32)
    own_rows = kv_index * seq_dev
    own_factor = lax.dynamic_slice_in_dim(row_factor, own_rows, seq_dev)[:, None]
    projected = projected * own_factor

    def split_heads(role_index):
        return projected[:, role_index * head_cols : (role_index + 1) * head_cols].reshape(
            seq_dev, heads_dev, head_size
        )

    query_vec = unit_rows(jax.nn.silu(split_heads(0))) * head_size ** (-0.5)
    key_vec = unit_rows(jax.nn.silu(split_heads(1)))
    value_vec = jax.nn.silu(split_heads(2))
    gate_vals = split_heads(3)
    head_start = tp_index * heads_dev

    def local_gate_values(values):
        own_seqs = lax.dynamic_slice_in_dim(values, own_rows, seq_dev, 0)
        return lax.dynamic_slice_in_dim(own_seqs, head_start, heads_dev, 1) * own_factor

    beta_gate = jax.nn.sigmoid(local_gate_values(beta_pre))
    decay_log_term = lax.dynamic_slice_in_dim(head_decay_log, head_start, heads_dev)
    decay_offset_term = lax.dynamic_slice_in_dim(decay_input_bias, head_start, heads_dev)
    head_decay_rate = jnp.exp(
        decay_extra_log
        - jnp.exp(decay_log_term)
        * jax.nn.softplus(local_gate_values(decay_logits) + decay_offset_term)
    )
    heads_f32, new_state = delta_step(
        query_vec, key_vec, value_vec, gate_vals, beta_gate, head_decay_rate, state, head_norm_gain
    )
    heads_out = heads_f32.reshape(seq_dev, head_cols).astype(jnp.bfloat16)
    mixer_terms = jnp.dot(
        lax.all_gather(heads_out, "kv", axis=0, tiled=True),
        mixer_output_weight,
        preferred_element_type=jnp.float32,
    )
    mixer_sum = lax.psum_scatter(
        mixer_terms.astype(jnp.bfloat16), "tp", scatter_dimension=1, tiled=True
    ).astype(jnp.float32)
    second_rows = (first32 + mixer_sum).astype(jnp.bfloat16)
    rows_last = lax.all_gather(second_rows, ("kv", "tp"), axis=1, tiled=True)
    last_terms = block_terms(
        rows_last, second_norm_gain, second_gate_weight, second_up_weight, second_down_weight
    )
    last_sum = lax.psum_scatter(
        last_terms.astype(jnp.bfloat16), ("kv", "tp"), scatter_dimension=1, tiled=True
    ).astype(jnp.float32)
    layer_out = (second_rows.astype(jnp.float32) + 0.5 * last_sum).astype(jnp.bfloat16)
    return (layer_out, new_state)


def solution(mesh):
    placed = (
        P("dp", ("kv", "tp")),
        P(),
        P(None, ("kv", "tp")),
        P(None, ("kv", "tp")),
        P(("kv", "tp"), None),
        P(),
        P("kv", "tp"),
        P("kv", "tp"),
        P("kv", "tp"),
        P("kv", "tp"),
        P(),
        P(),
        P(),
        P(),
        P(("dp", "kv"), "tp"),
        P(),
        P(("dp", "kv"), "tp", None, None),
        P("tp", "kv"),
        P(),
        P(None, ("kv", "tp")),
        P(None, ("kv", "tp")),
        P(("kv", "tp"), None),
    )
    return jax.shard_map(
        shards,
        mesh=mesh,
        in_specs=placed,
        out_specs=(P("dp", ("kv", "tp")), P(("dp", "kv"), "tp", None, None)),
        check_vma=False,
    )
```

profile of v0, /device:TPU:0, one launch (start us, length us, event | category | flops | bytes accessed | tf_op | source)
XLA Modules:
  0.0 181.2 jit_solution(4792796293112144642)
XLA Ops:
  7.2 16.1 %all_gather.12 = bf16[32,2048]{1,0:T(8,128)(2,1)S(1)} all-gather(bf16[32,256]{1,0:T(8,128)(2,1)} %param.22), channel_id=1, replica_groups=mesh['dp'=4,'kv'=4,'tp'=2] {'kv','tp'}, dimensions={1}, use_global_device_ids=true | all-gather | bytes 147456 | tf_op jit(solution)/shard_map/all_gather | solution.py:71
  24.0 3.4 %fusion.26 = f32[32,704]{1,0:T(8,128)} fusion(bf16[2048,704]{0,1:T(8,128)(2,1)} %param.24, bf16[32,2048]{1,0:T(8,128)(2,1)S(1)} %all_gather.12, f32[2048]{0:T(1024)} %param.23, f32[32]{0:T(128)S(1)} %add_rsqrt_fusion.5), kind=kOutput, calls=%fused_computation.41 | convolution fusion | flops 92536832 | bytes 3113088 | tf_op jit(solution)/shard_map/dot_general | solution.py:20
  27.4 4.3 %convolution_convert_fusion.1 = bf16[32,2048]{1,0:T(8,128)(2,1)} fusion(bf16[704,2048]{1,0:T(8,128)(2,1)S(1)} %copy-done, bf16[2048,704]{0,1:T(8,128)(2,1)} %param.25, f32[32,704]{1,0:T(8,128)} %fusion.26, bf16[32,2048]{1,0:T(8,128)(2,1)S(1)} %all_gather.12, f32[2048]{0:T(1024)} %param.23, f32[32]{0:T(128)} %copy-done.8), kind=kOutput, calls=%fused_computation.1 | convolution fusion | flops 185012224 | bytes 6127744 | tf_op jit(solution)/shard_map/dot_general | solution.py:23
  34.8 28.7 %reduce-scatter.5.cloned.1.call-done = bf16[32,256]{1,0:T(8,128)(2,1)} async-done(((bf16[32,2048]{1,0:T(8,128)(2,1)}), bf16[32,256]{1,0:T(8,128)(2,1)}) %reduce-scatter.5.cloned.1.call-update) | async-done | bytes 16400 | tf_op jit(solution)/shard_map/reduce_scatter | solution.py:75
  63.5 0.8 fusion.28
  64.3 1.8 %all_gather.13 = bf16[32,512]{1,0:T(8,128)(2,1)S(1)} all-gather(bf16[32,256]{1,0:T(8,128)(2,1)S(1)} %get-tuple-element.8), channel_id=1, replica_groups=mesh['dp'=4,'kv'=4,'tp'=2] {'tp'}, dimensions={1}, use_global_device_ids=true | all-gather | bytes 49152 | tf_op jit(solution)/shard_map/all_gather | solution.py:80
  66.2 0.8 fusion.43
  67.0 0.8 fusion.41
  68.0 1.2 convolution_convert_fusion.4
  69.2 1.2 convolution_convert_fusion.3
  70.5 1.3 convolution_convert_fusion.6
  72.5 14.4 %all-reduce = (f32[32]{0:T(128)S(1)}, f32[32,8]{0,1:T(8,128)S(1)}, f32[32,8]{0,1:T(8,128)S(1)}) all-reduce(f32[32]{0:T(128)S(1)} %get-tuple-element.7, f32[32,8]{0,1:T(8,128)S(1)} %fusion.43, f32[32,8]{0,1:T(8,128)S(1)} %fusion.41), channel_id=1, replica_groups=mesh['dp'=4,'kv'=4,'tp'=2] {'kv','tp'}, use_global_device_ids=true, to_apply=%region_4.5 | all-reduce | flops 544 | bytes 4352 | tf_op jit(solution)/shard_map/psum | solution.py:85
  87.1 3.0 %reduce-scatter.7.cloned.1.call-done = bf16[8,2048]{1,0:T(8,128)(2,1)} async-done(((bf16[32,2048]{1,0:T(8,128)(2,1)}), bf16[8,2048]{1,0:T(8,128)(2,1)}) %reduce-scatter.7.cloned.1.call-update) | async-done | bytes 32784 | tf_op jit(solution)/shard_map/reduce_scatter | solution.py:96
  90.1 1.0 convert_multiply_fusion.4
  91.4 3.4 %fusion.39 = f32[8,4,1,128]{3,2,1,0:T(1,128)S(1)} fusion(f32[8,4,128,128]{3,2,1,0:T(8,128)} %param.38, f32[8,4,128,1]{2,0,1,3:T(8,128)S(1)} %fusion.69), kind=kOutput, calls=%fused_computation.62 | convolution fusion | flops 6291456 | bytes 2129920 | tf_op jit(solution)/shard_map/shd,shde->she/dot_general | solution.py:29
  95.7 1.3 copy-done.2
  97.0 1.9 %fusion.37 = f32[8,4,1,128]{3,2,1,0:T(1,128)S(1)} fusion(f32[8,4,128,128]{3,2,1,0:T(8,128)S(1)} %multiply_add_fusion, f32[8,4,128,1]{2,0,1,3:T(8,128)S(1)} %get-tuple-element.9), kind=kOutput, calls=%fused_computation.60 | convolution fusion | flops 6291456 | bytes 2129920 | tf_op jit(solution)/shard_map/shd,shde->she/dot_general | solution.py:34
  99.1 13.1 %all_gather.14 = bf16[32,512]{1,0:T(8,128)(2,1)S(1)} all-gather(bf16[8,512]{1,0:T(8,128)(2,1)S(1)} %fusion.45), channel_id=1, replica_groups=mesh['dp'=4,'kv'=4,'tp'=2] {'kv'}, dimensions={0}, use_global_device_ids=true | all-gather | bytes 40960 | tf_op jit(solution)/shard_map/all_gather | solution.py:140
  113.1 5.8 %reduce-scatter.9.cloned.1.call-done = bf16[32,256]{1,0:T(8,128)(2,1)} async-done(((bf16[32,512]{1,0:T(8,128)(2,1)}), bf16[32,256]{1,0:T(8,128)(2,1)}) %reduce-scatter.9.cloned.1.call-update) | async-done | bytes 16400 | tf_op jit(solution)/shard_map/reduce_scatter | solution.py:144
  119.6 14.3 %all_gather.15 = bf16[32,2048]{1,0:T(8,128)(2,1)S(1)} all-gather(bf16[32,256]{1,0:T(8,128)(2,1)S(1)} %fusion.30), channel_id=1, replica_groups=mesh['dp'=4,'kv'=4,'tp'=2] {'kv','tp'}, dimensions={1}, use_global_device_ids=true | all-gather | bytes 147456 | tf_op jit(solution)/shard_map/all_gather | solution.py:148
  134.0 2.7 %fusion.22 = f32[32,704]{1,0:T(8,128)S(1)} fusion(bf16[2048,704]{0,1:T(8,128)(2,1)} %param.41, bf16[32,2048]{1,0:T(8,128)(2,1)S(1)} %all_gather.15, f32[2048]{0:T(1024)S(1)} %copy-done.6, f32[32]{0:T(128)S(1)} %add_rsqrt_fusion.3), kind=kOutput, calls=%fused_computation.40 | convolution fusion | flops 92536832 | bytes 3113088 | tf_op jit(solution)/shard_map/dot_general | solution.py:20
  136.7 5.1 %convolution_convert_fusion = bf16[32,2048]{1,0:T(8,128)(2,1)} fusion(bf16[704,2048]{1,0:T(8,128)(2,1)} %param.43, bf16[2048,704]{0,1:T(8,128)(2,1)} %param.42, f32[32,704]{1,0:T(8,128)S(1)} %fusion.22, bf16[32,2048]{1,0:T(8,128)(2,1)S(1)} %all_gather.15, f32[2048]{0:T(1024)S(1)} %copy-done.6, f32[32]{0:T(128)S(1)} %add_rsqrt_fusion.3), kind=kOutput, calls=%fused_computation | convolution fusion | flops 185012224 | bytes 6127744 | tf_op jit(solution)/shard_map/dot_general | solution.py:23
  141.9 31.5 %reduce-scatter.11.cloned.1.call-done = bf16[32,256]{1,0:T(8,128)(2,1)} async-done(((bf16[32,2048]{1,0:T(8,128)(2,1)}), bf16[32,256]{1,0:T(8,128)(2,1)}) %reduce-scatter.11.cloned.1.call-update) | async-done | bytes 16400 | tf_op jit(solution)/shard_map/reduce_scatter | solution.py:152
  173.4 1.3 add_convert_fusion
  (54 shorter events, 8.0 us)
Async XLA Ops:
  7.2 20.2 %copy-start = (bf16[704,2048]{1,0:T(8,128)(2,1)S(1)}, bf16[704,2048]{1,0:T(8,128)(2,1)}, u32[]{:S(2)}) copy-start(bf16[704,2048]{1,0:T(8,128)(2,1)} %param.26) | copy-start | bytes 8650756
  7.2 56.3 %reduce-scatter.5.cloned.1.call-start = ((), (), s32[]{:S(2)}) async-start(), calls=%async_computation.4 | async-start | bytes 147456 | tf_op jit(solution)/shard_map/reduce_scatter | solution.py:75
  23.5 0.5 copy-start.8
  27.4 36.2 %copy-start.5 = (bf16[32,256]{1,0:T(8,128)(2,1)S(1)}, bf16[32,256]{1,0:T(8,128)(2,1)}, u32[]{:S(2)}) copy-start(bf16[32,256]{1,0:T(8,128)(2,1)} %param.22) | copy-start | bytes 49156
  27.4 40.4 %copy-start.3 = (bf16[512,512]{1,0:T(8,128)(2,1)S(1)}, bf16[512,512]{1,0:T(8,128)(2,1)}, u32[]{:S(2)}) copy-start(bf16[512,512]{1,0:T(8,128)(2,1)} %param.29) | copy-start | bytes 1572868
  31.7 55.2 %copy-start.7 = (f32[8,4]{0,1:T(4,128)S(1)}, f32[8,4]{0,1:T(4,128)}, u32[]{:S(2)}) copy-start(f32[8,4]{0,1:T(4,128)} %param.36) | copy-start | bytes 388
  31.7 58.4 %reduce-scatter.7.cloned.1.call-start = ((), (), s32[]{:S(2)}) async-start(), calls=%async_computation.5 | async-start | bytes 163840 | tf_op jit(solution)/shard_map/reduce_scatter | solution.py:96
  72.4 46.4 %reduce-scatter.9.cloned.1.call-start = ((), (), s32[]{:S(2)}) async-start(), calls=%async_computation.6 | async-start | bytes 49152 | tf_op jit(solution)/shard_map/reduce_scatter | solution.py:144
  90.1 4.8 %copy-start.1 = (f32[8,4,128,128]{3,2,1,0:T(8,128)S(1)}, f32[8,4,128,128]{3,2,1,0:T(8,128)}, u32[]{:S(2)}) copy-start(f32[8,4,128,128]{3,2,1,0:T(8,128)} %param.38) | copy-start | bytes 6291460
  94.9 4.1 %copy-start.9 = (f32[128]{0:T(128)S(1)}, f32[128]{0:T(128)}, u32[]{:S(2)}) copy-start(f32[128]{0:T(128)} %param.37) | copy-start | bytes 1540
  94.9 17.3 %copy-start.4 = (bf16[512,512]{1,0:T(8,128)(2,1)S(1)}, bf16[512,512]{1,0:T(8,128)(2,1)}, u32[]{:S(2)}) copy-start(bf16[512,512]{1,0:T(8,128)(2,1)} %param.39) | copy-start | bytes 1572868
  94.9 39.1 %copy-start.6 = (f32[2048]{0:T(1024)S(1)}, f32[2048]{0:T(1024)}, u32[]{:S(2)}) copy-start(f32[2048]{0:T(1024)} %param.40) | copy-start | bytes 24580
  95.7 1.3 copy-start.2
  113.0 60.3 %reduce-scatter.11.cloned.1.call-start = ((), (), s32[]{:S(2)}) async-start(), calls=%async_computation.7 | async-start | bytes 147456 | tf_op jit(solution)/shard_map/reduce_scatter | solution.py:152
Sparse Core Ops, SparseCore 0:
  31.8 31.6 reduce-scatter.4
  72.5 17.5 reduce-scatter.6
  113.2 5.6 reduce-scatter.8
  142.0 31.3 reduce-scatter.10
where the time goes:
time: 182 us; the launch traced here: 181 us
  waiting for transfers between devices  69.1 us (38%)
  blocking collectives  59.7 us (33%)
  matrix products  27.2 us (15%)
  between operations  13.9 us (8%)
  other arithmetic  6.18 us (3%)
  local copies, waits for them, and re-layouts  5.02 us (3%)
    reduce_scatter x1, waiting for transfers between devices, shards(): lax.psum_scatter(last_terms.astype(jnp.bfloat16), ('kv', 'tp'), scatter_d...  31.5 us
    reduce_scatter x1, waiting for transfers between devices, shards(): lax.psum_scatter(ffn_terms.astype(jnp.bfloat16), ('kv', 'tp'), scatter_di...  28.7 us
    all_gather x1, blocking collectives, shards(): rows_all = lax.all_gather(tokens, ('kv', 'tp'), axis=1, tiled=True)  16.1 us
    psum x1, blocking collectives, shards(): lax.psum((jnp.sum(first32 * first32, axis=1), jnp.dot(own_scaled, beta_ro...  14.4 us
    all_gather x1, blocking collectives, shards(): rows_last = lax.all_gather(second_rows, ('kv', 'tp'), axis=1, tiled=True)  14.3 us
    all_gather x1, blocking collectives, shards(): lax.all_gather(heads_out, 'kv', axis=0, tiled=True)  13.1 us
    dot_general x2, matrix products, block_terms(): return jnp.dot(hidden, w_down, preferred_element_type=jnp.float32)  9.45 us
    dot_general x2, matrix products, block_terms(): gate_pre = jnp.dot(normed, w_gate, preferred_element_type=jnp.float32)  6.1 us
  transfers between devices with their start and end apart: 4, of which 4 were waited for; matrix products, arithmetic and copies ran while one was open for 2% of the time, Pallas kernels for 0%

commit v1 on v0

--- a/solution.py
+++ b/solution.py
@@ -68,7 +68,7 @@
     kv_width = query_weight.shape[0]
     head_cols = heads_dev * head_size
     model_width = mixer_norm_gain.shape[0]
-    rows_all = lax.all_gather(tokens, ("kv", "tp"), axis=1, tiled=True)
+    rows_all = jnp.concatenate(lax.all_gather(tokens, ("kv", "tp")), axis=1)
     ffn_terms = block_terms(
         rows_all, first_norm_gain, first_gate_weight, first_up_weight, first_down_weight
     )

time: 182 us -> 182 us (level)
  transfers between devices with their start and end apart: 4 -> 4, of which waited for: 4 -> 4; matrix products, arithmetic and copies ran while one was open for 2% -> 1% of each run, Pallas kernels for 0% -> 0%
where the time goes in v1:
time: 182 us; the launch traced here: 181 us
  waiting for transfers between devices  70.5 us (39%)
  blocking collectives  59.7 us (33%)
  matrix products  27.5 us (15%)
  between operations  14 us (8%)
  other arithmetic  6.2 us (3%)
  local copies, waits for them, and re-layouts  3.26 us (2%)
    reduce_scatter x1, waiting for transfers between devices, shards(): lax.psum_scatter(last_terms.astype(jnp.bfloat16), ('kv', 'tp'), scatter_d...  31.6 us
    reduce_scatter x1, waiting for transfers between devices, shards(): lax.psum_scatter(ffn_terms.astype(jnp.bfloat16), ('kv', 'tp'), scatter_di...  30 us
    all_gather x1, blocking collectives, shards(): rows_all = jnp.concatenate(lax.all_gather(tokens, ('kv', 'tp')), axis=1)  16.1 us
    psum x1, blocking collectives, shards(): lax.psum((jnp.sum(first32 * first32, axis=1), jnp.dot(own_scaled, beta_ro...  14.5 us
    all_gather x1, blocking collectives, shards(): rows_last = lax.all_gather(second_rows, ('kv', 'tp'), axis=1, tiled=True)  14.2 us
    all_gather x1, blocking collectives, shards(): lax.all_gather(heads_out, 'kv', axis=0, tiled=True)  13.1 us
    dot_general x2, matrix products, block_terms(): return jnp.dot(hidden, w_down, preferred_element_type=jnp.float32)  9.37 us
    reduce_scatter x1, waiting for transfers between devices, shards(): lax.psum_scatter(mixer_terms.astype(jnp.bfloat16), 'tp', scatter_dimensio...  5.75 us
  transfers between devices with their start and end apart: 4, of which 4 were waited for; matrix products, arithmetic and copies ran while one was open for 1% of the time, Pallas kernels for 0%

profile of v1, /device:TPU:0, one launch (start us, length us, event | category | flops | bytes accessed | tf_op | source)
XLA Modules:
  0.0 181.3 jit_solution(7438528477165620359)
XLA Ops:
  7.2 16.1 %all-gather = bf16[256,256]{1,0:T(8,128)(2,1)S(1)} all-gather(bf16[32,256]{1,0:T(8,128)(2,1)} %param.22), channel_id=2, replica_groups=mesh['dp'=4,'kv'=4,'tp'=2] {'kv','tp'}, dimensions={0}, use_global_device_ids=true | all-gather | bytes 147456 | tf_op jit(solution)/shard_map/all_gather | solution.py:71
  23.5 2.7 %fusion.48 = f32[32,704]{1,0:T(8,128)S(1)} fusion(bf16[2048,704]{0,1:T(8,128)(2,1)} %param.24, f32[32,2048]{1,0:T(8,128)S(1)} %bitcast.77, f32[2048]{0:T(1024)} %param.23, f32[32]{0:T(128)S(1)} %add_rsqrt_fusion.5), kind=kOutput, calls=%fused_computation.88 | convolution fusion | flops 92471296 | bytes 3244160 | tf_op jit(solution)/shard_map/dot_general | solution.py:20
  26.3 4.3 %convolution_convert_fusion.1 = bf16[32,2048]{1,0:T(8,128)(2,1)} fusion(bf16[704,2048]{1,0:T(8,128)(2,1)S(1)} %copy-done, bf16[2048,704]{0,1:T(8,128)(2,1)} %param.25, f32[32,704]{1,0:T(8,128)S(1)} %fusion.48, f32[32,2048]{1,0:T(8,128)S(1)} %bitcast.78, f32[2048]{0:T(1024)S(1)} %copy-done.5, f32[32]{0:T(128)S(1)} %add_rsqrt_fusion.5), kind=kOutput, calls=%fused_computation.1 | convolution fusion | flops 184946688 | bytes 6258816 | tf_op jit(solution)/shard_map/dot_general | solution.py:23
  32.4 30.0 %reduce-scatter.5.cloned.1.call-done = bf16[32,256]{1,0:T(8,128)(2,1)} async-done(((bf16[32,2048]{1,0:T(8,128)(2,1)}), bf16[32,256]{1,0:T(8,128)(2,1)}) %reduce-scatter.5.cloned.1.call-update) | async-done | bytes 16400 | tf_op jit(solution)/shard_map/reduce_scatter | solution.py:75
  62.4 0.8 fusion.21
  63.2 1.8 %all_gather.17 = bf16[32,512]{1,0:T(8,128)(2,1)S(1)} all-gather(bf16[32,256]{1,0:T(8,128)(2,1)S(1)} %get-tuple-element.8), channel_id=1, replica_groups=mesh['dp'=4,'kv'=4,'tp'=2] {'tp'}, dimensions={1}, use_global_device_ids=true | all-gather | bytes 49152 | tf_op jit(solution)/shard_map/all_gather | solution.py:80
  65.8 0.8 fusion.34
  66.7 1.2 convolution_convert_fusion.5
  67.9 1.2 convolution_convert_fusion.4
  69.1 1.2 convolution_convert_fusion.3
  70.4 1.3 convolution_convert_fusion.6
  72.4 14.5 %all-reduce = (f32[32]{0:T(128)S(1)}, f32[32,8]{0,1:T(8,128)S(1)}, f32[32,8]{0,1:T(8,128)S(1)}) all-reduce(f32[32]{0:T(128)S(1)} %get-tuple-element.7, f32[32,8]{0,1:T(8,128)S(1)} %fusion.36, f32[32,8]{0,1:T(8,128)S(1)} %fusion.34), channel_id=1, replica_groups=mesh['dp'=4,'kv'=4,'tp'=2] {'kv','tp'}, use_global_device_ids=true, to_apply=%region_4.5 | all-reduce | flops 544 | bytes 4352 | tf_op jit(solution)/shard_map/psum | solution.py:85
  87.1 3.0 %reduce-scatter.7.cloned.1.call-done = bf16[8,2048]{1,0:T(8,128)(2,1)} async-done(((bf16[32,2048]{1,0:T(8,128)(2,1)}), bf16[8,2048]{1,0:T(8,128)(2,1)}) %reduce-scatter.7.cloned.1.call-update) | async-done | bytes 32784 | tf_op jit(solution)/shard_map/reduce_scatter | solution.py:96
  90.1 1.0 convert_multiply_fusion.2
  91.4 3.4 %fusion.32 = f32[8,4,1,128]{3,2,1,0:T(1,128)S(1)} fusion(f32[8,4,128,128]{3,2,1,0:T(8,128)} %param.38, f32[8,4,128,1]{2,0,1,3:T(8,128)S(1)} %fusion.64), kind=kOutput, calls=%fused_computation.58 | convolution fusion | flops 6291456 | bytes 2129920 | tf_op jit(solution)/shard_map/shd,shde->she/dot_general | solution.py:29
  95.7 1.3 copy-done.2
  97.0 1.9 %fusion.30 = f32[8,4,1,128]{3,2,1,0:T(1,128)S(1)} fusion(f32[8,4,128,128]{3,2,1,0:T(8,128)S(1)} %multiply_add_fusion, f32[8,4,128,1]{2,0,1,3:T(8,128)S(1)} %get-tuple-element.9), kind=kOutput, calls=%fused_computation.56 | convolution fusion | flops 6291456 | bytes 2129920 | tf_op jit(solution)/shard_map/shd,shde->she/dot_general | solution.py:34
  99.1 13.1 %all_gather.18 = bf16[32,512]{1,0:T(8,128)(2,1)S(1)} all-gather(bf16[8,512]{1,0:T(8,128)(2,1)S(1)} %fusion.38), channel_id=1, replica_groups=mesh['dp'=4,'kv'=4,'tp'=2] {'kv'}, dimensions={0}, use_global_device_ids=true | all-gather | bytes 40960 | tf_op jit(solution)/shard_map/all_gather | solution.py:140
  113.1 5.8 %reduce-scatter.9.cloned.1.call-done = bf16[32,256]{1,0:T(8,128)(2,1)} async-done(((bf16[32,512]{1,0:T(8,128)(2,1)}), bf16[32,256]{1,0:T(8,128)(2,1)}) %reduce-scatter.9.cloned.1.call-update) | async-done | bytes 16400 | tf_op jit(solution)/shard_map/reduce_scatter | solution.py:144
  119.5 14.2 %all_gather.19 = bf16[32,2048]{1,0:T(8,128)(2,1)S(1)} all-gather(bf16[32,256]{1,0:T(8,128)(2,1)S(1)} %fusion.23), channel_id=1, replica_groups=mesh['dp'=4,'kv'=4,'tp'=2] {'kv','tp'}, dimensions={1}, use_global_device_ids=true | all-gather | bytes 147456 | tf_op jit(solution)/shard_map/all_gather | solution.py:148
  133.9 2.7 %fusion.19 = f32[32,704]{1,0:T(8,128)S(1)} fusion(bf16[2048,704]{0,1:T(8,128)(2,1)} %param.41, bf16[32,2048]{1,0:T(8,128)(2,1)S(1)} %all_gather.19, f32[2048]{0:T(1024)S(1)} %copy-done.6, f32[32]{0:T(128)S(1)} %add_rsqrt_fusion.3), kind=kOutput, calls=%fused_computation.37 | convolution fusion | flops 92536832 | bytes 3113088 | tf_op jit(solution)/shard_map/dot_general | solution.py:20
  136.6 5.1 %convolution_convert_fusion = bf16[32,2048]{1,0:T(8,128)(2,1)} fusion(bf16[704,2048]{1,0:T(8,128)(2,1)} %param.43, bf16[2048,704]{0,1:T(8,128)(2,1)} %param.42, f32[32,704]{1,0:T(8,128)S(1)} %fusion.19, bf16[32,2048]{1,0:T(8,128)(2,1)S(1)} %all_gather.19, f32[2048]{0:T(1024)S(1)} %copy-done.6, f32[32]{0:T(128)S(1)} %add_rsqrt_fusion.3), kind=kOutput, calls=%fused_computation | convolution fusion | flops 185012224 | bytes 6127744 | tf_op jit(solution)/shard_map/dot_general | solution.py:23
  141.8 31.6 %reduce-scatter.11.cloned.1.call-done = bf16[32,256]{1,0:T(8,128)(2,1)} async-done(((bf16[32,2048]{1,0:T(8,128)(2,1)}), bf16[32,256]{1,0:T(8,128)(2,1)}) %reduce-scatter.11.cloned.1.call-update) | async-done | bytes 16400 | tf_op jit(solution)/shard_map/reduce_scatter | solution.py:152
  173.4 1.3 add_convert_fusion
  (58 shorter events, 6.8 us)
Async XLA Ops:
  7.2 19.1 %copy-start = (bf16[704,2048]{1,0:T(8,128)(2,1)S(1)}, bf16[704,2048]{1,0:T(8,128)(2,1)}, u32[]{:S(2)}) copy-start(bf16[704,2048]{1,0:T(8,128)(2,1)} %param.26) | copy-start | bytes 8650756
  7.2 19.1 %copy-start.5 = (f32[2048]{0:T(1024)S(1)}, f32[2048]{0:T(1024)}, u32[]{:S(2)}) copy-start(f32[2048]{0:T(1024)} %param.23) | copy-start | bytes 24580
  7.2 55.2 %reduce-scatter.5.cloned.1.call-start = ((), (), s32[]{:S(2)}) async-start(), calls=%async_computation.4 | async-start | bytes 147456 | tf_op jit(solution)/shard_map/reduce_scatter | solution.py:75
  26.3 4.4 %copy-start.9 = (f32[8]{0:T(128)S(1)}, f32[8]{0:T(128)}, u32[]{:S(2)}) copy-start(f32[8]{0:T(128)} %param.35) | copy-start | bytes 100
  26.3 6.0 %copy-start.10 = (f32[8]{0:T(128)S(1)}, f32[8]{0:T(128)}, u32[]{:S(2)}) copy-start(f32[8]{0:T(128)} %param.34) | copy-start | bytes 100
  26.3 36.1 %copy-start.4 = (bf16[32,256]{1,0:T(8,128)(2,1)S(1)}, bf16[32,256]{1,0:T(8,128)(2,1)}, u32[]{:S(2)}) copy-start(bf16[32,256]{1,0:T(8,128)(2,1)} %param.22) | copy-start | bytes 49156
  30.6 56.3 %copy-start.7 = (f32[8,4]{0,1:T(4,128)S(1)}, f32[8,4]{0,1:T(4,128)}, u32[]{:S(2)}) copy-start(f32[8,4]{0,1:T(4,128)} %param.36) | copy-start | bytes 388
  30.6 59.5 %reduce-scatter.7.cloned.1.call-start = ((), (), s32[]{:S(2)}) async-start(), calls=%async_computation.5 | async-start | bytes 163840 | tf_op jit(solution)/shard_map/reduce_scatter | solution.py:96
  72.3 46.5 %reduce-scatter.9.cloned.1.call-start = ((), (), s32[]{:S(2)}) async-start(), calls=%async_computation.6 | async-start | bytes 49152 | tf_op jit(solution)/shard_map/reduce_scatter | solution.py:144
  90.1 4.8 %copy-start.1 = (f32[8,4,128,128]{3,2,1,0:T(8,128)S(1)}, f32[8,4,128,128]{3,2,1,0:T(8,128)}, u32[]{:S(2)}) copy-start(f32[8,4,128,128]{3,2,1,0:T(8,128)} %param.38) | copy-start | bytes 6291460
  94.9 4.1 %copy-start.8 = (f32[128]{0:T(128)S(1)}, f32[128]{0:T(128)}, u32[]{:S(2)}) copy-start(f32[128]{0:T(128)} %param.37) | copy-start | bytes 1540
  94.9 17.3 %copy-start.3 = (bf16[512,512]{1,0:T(8,128)(2,1)S(1)}, bf16[512,512]{1,0:T(8,128)(2,1)}, u32[]{:S(2)}) copy-start(bf16[512,512]{1,0:T(8,128)(2,1)} %param.39) | copy-start | bytes 1572868
  94.9 39.0 %copy-start.6 = (f32[2048]{0:T(1024)S(1)}, f32[2048]{0:T(1024)}, u32[]{:S(2)}) copy-start(f32[2048]{0:T(1024)} %param.40) | copy-start | bytes 24580
  95.7 1.3 copy-start.2
  113.0 60.4 %reduce-scatter.11.cloned.1.call-start = ((), (), s32[]{:S(2)}) async-start(), calls=%async_computation.7 | async-start | bytes 147456 | tf_op jit(solution)/shard_map/reduce_scatter | solution.py:152
Sparse Core Ops, SparseCore 0:
  30.7 31.5 reduce-scatter.4
  72.4 17.6 reduce-scatter.6
  113.1 5.6 reduce-scatter.8
  141.9 31.4 reduce-scatter.10
